TPU v7x, 32 devices: a whole 2x2x4 slice. The times are simulated.
32 devices in a mesh: sp: 8 (over z, y), tp: 4 (over x, core).
Axes of the slice: x: 2, y: 2, z: 4, core: 2. Of those that a mesh axis runs over, the one named last changes fastest.
Arguments:
- queries: bfloat16 [8192, 1024], P('sp', 'tp'), may hold values from -6 to 6
- cell_key_rows: bfloat16 [8192, 1024], P('sp', 'tp'), may hold values from -6 to 6
- cell_value_rows: bfloat16 [8192, 2048], P('sp', 'tp'), may hold values from -6 to 6
- output_gate_logits: bfloat16 [8192, 2048], P('sp', 'tp'), may hold values from -6 to 6
- input_gate_logits: bfloat16 [8, 8192], P('tp', 'sp'), may hold values from -4 to 216
- forget_gate_logits: bfloat16 [8, 8192], P('tp', 'sp'), may hold values from 0.5 to 14
- forget_extra_term: float32 [8, 8192], P('tp', 'sp'), may hold values from -1.4 to 0
- residual: bfloat16 [8192, 2048], P('sp', 'tp'), may hold values from -13 to 13
- head_norm_gain: bfloat16 [2048], P('tp'), may hold values from 0.099609375 to 1.8984375
- cell_output_weight: bfloat16 [2048, 2048], P('tp'), may hold values from -0.25 to 0.25
- feedforward_norm_gain: bfloat16 [2048], replicated, may hold values from 0.099609375 to 1.8984375
- gate_projection_weight: bfloat16 [2048, 5632], P('sp', 'tp'), may hold values from -0.125 to 0.125
- up_projection_weight: bfloat16 [2048, 5632], P('sp', 'tp'), may hold values from -0.125 to 0.125
- down_projection_weight: bfloat16 [5632, 2048], P('tp', 'sp'), may hold values from -0.15625 to 0.15625
Outputs:
- mixed: bfloat16 [8192, 2048], P('sp', 'tp')
All inputs are finite; a program needn't handle non-finite values.
Results may differ from a plain program's by a relative error of at most 0.017.
Values may be sent and summed in bfloat16 or wider, within the bound.
A program may use at most 128 MiB of HBM per device.

v0:
```python
import jax
import jax.numpy as jnp
from jax import lax
from jax.sharding import PartitionSpec as P

PRECISE = lax.Precision.HIGHEST
LOWEST_LOG = -1e30
EPSILON = 1e-06


def entering(array, axis, combine, identity):
    length, index = (lax.axis_size(axis), lax.axis_index(axis))
    everything = jax.tree.map(lambda part: lax.all_gather(part, axis), array)
    start = jax.tree.map(
        lambda part, zero: jnp.broadcast_to(jnp.asarray(zero, part.dtype), part.shape),
        array,
        identity,
    )

    def step(k, before):
        reached = k < index
        new = combine(before, jax.tree.map(lambda part: part[k], everything))
        return jax.tree.map(lambda a, b: jnp.where(reached, a, b), new, before)

    return lax.fori_loop(0, length, step, start)


def to_blocks(array, block_count, block_size):
    shaped = array.reshape((array.shape[0], block_count, block_size) + array.shape[2:])
    return jnp.moveaxis(shaped, 1, 0)


def from_blocks(array):
    moved = jnp.moveaxis(array, 0, 1)
    return moved.reshape((moved.shape[0], moved.shape[1] * moved.shape[2]) + moved.shape[3:])


def memory_blocks(
    query_raw, key_raw, value_heads, in_gates, forget_log_value, block_size, query_scale
):
    head_count, length, key_width = query_raw.shape
    value_width = value_heads.shape[2]
    block_count = length // block_size
    causal = jnp.tril(jnp.ones((block_size, block_size), bool))

    def advance(carried, pieces):
        memory_state, top_log, offset = carried
        query_block, key_block, value_block, gate_block, forget_block = pieces
        running = jnp.cumsum(forget_block, axis=-1)
        log_weight = jnp.where(
            causal, running[:, :, None] - running[:, None, :] + gate_block[:, None, :], -jnp.inf
        )
        log_start = running + top_log[:, None]
        row_max = jnp.maximum(jnp.max(log_weight, axis=-1), log_start)
        scores = jnp.einsum(
            "htd,hsd->hts", query_block, key_block, preferred_element_type=jnp.float32
        )
        scores = scores * query_scale * jnp.exp(log_weight - row_max[:, :, None])
        query_wide = query_block.astype(jnp.float32) * query_scale
        earlier = jnp.einsum("htd,hde->hte", query_wide, memory_state, precision=PRECISE)
        numerator = jnp.exp(log_start - row_max)[:, :, None] * earlier
        numerator = numerator + jnp.einsum("hts,hse->hte", scores, value_block, precision=PRECISE)
        last_cum = running[:, -1]
        log_end = last_cum[:, None] - running + gate_block
        new_top = jnp.maximum(last_cum + top_log, jnp.max(log_end, axis=-1))
        scaled = key_block.astype(jnp.float32) * jnp.exp(log_end - new_top[:, None])[:, :, None]
        memory_state = jnp.exp(last_cum + top_log - new_top)[:, None, None] * memory_state
        memory_state = memory_state + jnp.einsum(
            "hsd,hse->hde", scaled, value_block, precision=PRECISE
        )
        return (
            (memory_state, new_top, offset + last_cum),
            (numerator, row_max, offset[:, None] + running),
        )

    initial = (
        jnp.zeros((head_count, key_width, value_width), jnp.float32),
        jnp.full((head_count,), LOWEST_LOG, jnp.float32),
        jnp.zeros((head_count,), jnp.float32),
    )
    pieces = tuple(
        (
            to_blocks(array, block_count, block_size)
            for array in (query_raw, key_raw, value_heads, in_gates, forget_log_value)
        )
    )
    ending, outputs = lax.scan(advance, initial, pieces)
    return (tuple((from_blocks(output) for output in outputs)), ending)


def join_states(earlier, later):
    state_early, top_early, total_early = earlier
    state_late, top_late, total_late = later
    moved_top = top_early + total_late
    new_top = jnp.maximum(moved_top, top_late)
    joined = jnp.exp(moved_top - new_top)[:, None, None] * state_early
    joined = joined + jnp.exp(top_late - new_top)[:, None, None] * state_late
    return (joined, new_top, total_early + total_late)


def heads_first(array, head_count):
    token_rows = array.shape[0]
    width = array.shape[1] // head_count
    return jnp.transpose(array.reshape(token_rows, head_count, width), (1, 0, 2))


def local(
    queries,
    cell_key_rows,
    cell_value_rows,
    output_gate_logits,
    input_gate_logits,
    forget_gate_logits,
    forget_extra_term,
    residual,
    head_norm_gain,
    cell_output_weight,
    feedforward_norm_gain,
    gate_projection_weight,
    up_projection_weight,
    down_projection_weight,
):
    whole_gate, whole_up, whole_down = (
        lax.all_gather(gate_projection_weight, "sp", axis=0, tiled=True),
        lax.all_gather(up_projection_weight, "sp", axis=0, tiled=True),
        lax.all_gather(down_projection_weight, "sp", axis=1, tiled=True),
    )
    token_rows = queries.shape[0]
    head_count = input_gate_logits.shape[0]
    key_width = queries.shape[1] // head_count
    value_width = cell_value_rows.shape[1] // head_count
    query_scale = key_width ** (-0.5)
    query_raw = heads_first(queries, head_count)
    key_raw = heads_first(cell_key_rows, head_count)
    value_heads = heads_first(cell_value_rows, head_count).astype(jnp.float32)
    forget_log_value = (
        jax.nn.log_sigmoid(forget_gate_logits.astype(jnp.float32)) + forget_extra_term
    )
    results, ending = memory_blocks(
        query_raw,
        key_raw,
        value_heads,
        input_gate_logits.astype(jnp.float32),
        forget_log_value,
        min(token_rows, 512),
        query_scale,
    )
    numerator, local_max, offsets = results
    end_state, end_top, end_total = ending
    identity = (
        jnp.zeros_like(end_state),
        jnp.full_like(end_top, LOWEST_LOG),
        jnp.zeros_like(end_total),
    )
    carried_state, carried_top, _ = entering(
        (end_state, end_top, end_total), "sp", join_states, identity
    )
    shifted = offsets + carried_top[:, None]
    row_max = jnp.maximum(local_max, shifted)
    query_heads = query_raw.astype(jnp.float32) * query_scale
    from_before = jnp.einsum("htd,hde->hte", query_heads, carried_state, precision=PRECISE)
    memory = (
        jnp.exp(local_max - row_max)[:, :, None] * numerator
        + jnp.exp(shifted - row_max)[:, :, None] * from_before
    )
    memory = jnp.transpose(memory, (1, 0, 2))
    normal = memory * lax.rsqrt(jnp.mean(memory * memory, axis=-1, keepdims=True) + EPSILON)
    gate_open = jax.nn.sigmoid(
        output_gate_logits.astype(jnp.float32).reshape(token_rows, head_count, value_width)
    )
    gated_heads = (
        normal * head_norm_gain.astype(jnp.float32).reshape(head_count, value_width) * gate_open
    )
    gated_heads = gated_heads.reshape(token_rows, head_count * value_width).astype(jnp.bfloat16)
    partial_value = jnp.dot(
        gated_heads, cell_output_weight, preferred_element_type=jnp.float32
    ).astype(jnp.bfloat16)
    column_count = residual.shape[1]
    column_start = lax.axis_index("tp") * column_count
    summed = lax.psum_scatter(partial_value, "tp", scatter_dimension=1, tiled=True).astype(
        jnp.float32
    )
    stream = (residual.astype(jnp.float32) + summed).astype(jnp.bfloat16)
    stream_local = stream.astype(jnp.float32)
    squares = lax.psum(jnp.sum(stream_local * stream_local, axis=1), "tp")
    scale = lax.rsqrt(squares / feedforward_norm_gain.shape[0] + EPSILON)[:, None]
    gain_columns = lax.dynamic_slice_in_dim(
        feedforward_norm_gain, column_start, column_count, 0
    ).astype(jnp.float32)
    normed = lax.all_gather(
        (stream_local * scale * gain_columns).astype(jnp.bfloat16), "tp", axis=1, tiled=True
    )
    gate_value = jnp.dot(normed, whole_gate, preferred_element_type=jnp.float32)
    lifted = jnp.dot(normed, whole_up, preferred_element_type=jnp.float32)
    hidden = (jax.nn.silu(gate_value) * lifted).astype(jnp.bfloat16)
    down_terms = jnp.dot(hidden, whole_down, preferred_element_type=jnp.float32)
    channel_total = lax.psum_scatter(
        down_terms.astype(jnp.bfloat16), "tp", scatter_dimension=1, tiled=True
    ).astype(jnp.float32)
    return (stream.astype(jnp.float32) + 0.5 * channel_total).astype(jnp.bfloat16)


def solution(mesh):
    placed = (
        P("sp", "tp"),
        P("sp", "tp"),
        P("sp", "tp"),
        P("sp", "tp"),
        P("tp", "sp"),
        P("tp", "sp"),
        P("tp", "sp"),
        P("sp", "tp"),
        P("tp"),
        P("tp", None),
        P(),
        P("sp", "tp"),
        P("sp", "tp"),
        P("tp", "sp"),
    )
    return jax.shard_map(
        local, mesh=mesh, in_specs=placed, out_specs=P("sp", "tp"), check_vma=False
    )
```

profile of v0, /device:TPU:0, one launch (start us, length us, event | category | flops | bytes accessed | tf_op | source)
XLA Modules:
  0.0 540.1 jit_solution(7199471552716918428)
XLA Ops:
  6.6 1.4 copy.44
  8.0 1.0 copy.45
  9.0 2.3 copy.42
  11.2 2.8 convert_bitcast_fusion
  14.1 2.9 copy.43
  17.0 1.3 copy.40
  18.3 0.3 copy.41
  18.6 18.4 %while.37 = (s32[]{:T(128)}, f32[2,128,256]{2,1,0:T(8,128)S(1)}, f32[2]{0:T(128)S(1)}, f32[2]{0:T(128)S(1)}, f32[2,2,512,256]{3,2,1,0:T(8,128)}, /*index=5*/f32[...) while((s32[]{:T(128)}, f32[2,128,256]{2,1,0:T(8,128)S(1)}, ...), condition=%wide.region_5.6_spmd.clone, body=%wide.region_0.5_spmd.clone.sunk | while | flops 2557093888 | bytes 39478384 | solution.py:87
  18.7 0.6 reduce-window.14
  19.5 0.2 reduce-window.15
  19.7 0.2 slice_reduce_fusion.5
  19.9 0.2 fusion.118
  20.2 0.7 fusion.121
  21.0 1.5 fusion.120
  22.5 2.6 fusion.122
  25.2 1.1 fusion.123
  26.4 1.3 convolution_add_fusion.2
  27.9 0.6 reduce-window.14
  28.9 0.2 slice_reduce_fusion.5
  29.1 0.2 fusion.118
  29.4 0.7 fusion.121
  30.1 1.5 fusion.120
  31.7 2.6 fusion.122
  34.4 1.1 fusion.123
  35.6 1.3 convolution_add_fusion.2
  37.0 0.7 copy-done.2
  37.8 0.6 dynamic-slice
  39.0 0.2 dynamic-update-slice
  39.3 0.2 dynamic-update-slice.1
  39.5 23.3 %all-reduce.2 = (f32[16]{0:T(128)S(1)}, f32[16]{0:T(128)S(1)}) all-reduce(f32[16]{0:T(128)S(1)} %dynamic-update-slice, f32[16]{0:T(128)S(1)} %dynamic-update-slice.1), channel_id=2, replica_groups=mesh['sp'=8,'tp'=4] {'sp'}, use_global_device_ids=true, to_apply=%add | all-reduce | flops 32 | bytes 256
  63.0 4.2 copy.49
  67.1 4.2 reshape.321
  71.3 1.9 add_divide_fusion
  73.2 2.9 copy.52
  76.1 13.6 %all-gather.17.cloned.1.call-done = f32[16,128,256]{2,1,0:T(8,128)} async-done(((f32[2,128,256]{2,1,0:T(8,128)}), f32[16,128,256]{2,1,0:T(8,128)}) %all-gather.17.cloned.1.call-update) | async-done | bytes 2097168 | tf_op jit(solution)/shard_map/all_gather | solution.py:13
  89.8 9.1 %while.38 = (s32[]{:T(128)}, f32[2,128,256]{2,1,0:T(8,128)S(1)}, f32[2]{0:T(128)S(1)}, s32[]{:T(128)}, f32[8,2]{1,0:T(8,128)S(1)}, /*index=5*/f32[8,2]{1,0:T(8,1...) while((s32[]{:T(128)}, f32[2,128,256]{2,1,0:T(8,128)S(1)}, f32[2]{0:T(128)S(1)}, s32[]{:T(128)}, ...), condition=%wide.region_7.8_spmd.clone, body=%wide.region_6.7_spmd.clone.sunk | while | flops 327698 | bytes 786647 | solution.py:25
  89.8 1.1 fusion.124
  91.0 1.1 fusion.124
  92.1 1.1 fusion.124
  93.3 1.1 fusion.124
  94.4 1.1 fusion.124
  95.5 1.1 fusion.124
  96.6 1.1 fusion.124
  97.8 1.1 fusion.124
  99.0 3.9 fusion.58
  102.9 0.3 fusion.61
  103.2 4.4 convolution_convert_fusion.1
  107.7 0.7 all-gather.11.cloned.1.call-update
  108.5 0.8 dynamic-slice_convert_fusion
  109.2 41.6 %reduce-scatter.3.cloned.1.call-done = bf16[1024,512]{1,0:T(8,128)(2,1)} async-done(((bf16[1024,2048]{1,0:T(8,128)(2,1)}), bf16[1024,512]{1,0:T(8,128)(2,1)}) %reduce-scatter.3.cloned.1.call-update) | async-done | bytes 1048592 | tf_op jit(solution)/shard_map/reduce_scatter | solution.py:180
  150.8 1.7 fusion.54
  152.5 5.8 %psum.7 = f32[1024]{0:T(1024)S(1)} all-reduce(f32[1024]{0:T(1024)S(1)} %fusion.54), channel_id=1, replica_groups=mesh['sp'=8,'tp'=4] {'tp'}, use_global_device_ids=true, to_apply=%region_11.12 | all-reduce | flops 1024 | bytes 8192 | tf_op jit(solution)/shard_map/psum | solution.py:185
  158.3 1.4 fusion.56
  159.7 0.5 all-gather.13.cloned.1.call-update
  160.3 0.5 all-gather.15.cloned.1.call-update
  160.9 0.3 reduce-scatter.5.cloned.1.call-start
  161.1 84.2 %all-gather.11.cloned.1.call-done = bf16[2048,1408]{1,0:T(8,128)(2,1)} async-done(((bf16[256,1408]{1,0:T(8,128)(2,1)}), bf16[2048,1408]{1,0:T(8,128)(2,1)}) %all-gather.11.cloned.1.call-update) | async-done | bytes 5767184 | tf_op jit(solution)/shard_map/all_gather | solution.py:124
  245.3 34.1 %all-gather.9.cloned.1.call-done = bf16[1024,2048]{1,0:T(8,128)(2,1)} async-done(((bf16[1024,512]{1,0:T(8,128)(2,1)}), bf16[1024,2048]{1,0:T(8,128)(2,1)}) %all-gather.9.cloned.1.call-update) | async-done | bytes 4194320 | tf_op jit(solution)/shard_map/all_gather | solution.py:190
  279.4 11.7 %fusion.74 = f32[1024,1408]{1,0:T(8,128)} fusion(bf16[1024,2048]{1,0:T(8,128)(2,1)} %all-gather.9.cloned.1.call-done, bf16[2048,1408]{1,0:T(8,128)(2,1)} %all-gather.11.cloned.1.call-done), kind=kOutput, calls=%fused_computation.117 | convolution fusion | flops 5905580032 | bytes 15728640 | tf_op jit(solution)/shard_map/dot_general | solution.py:193
  291.1 82.7 %all-gather.13.cloned.1.call-done = bf16[2048,1408]{1,0:T(8,128)(2,1)} async-done(((bf16[256,1408]{1,0:T(8,128)(2,1)}), bf16[2048,1408]{1,0:T(8,128)(2,1)}) %all-gather.13.cloned.1.call-update) | async-done | bytes 5767184 | tf_op jit(solution)/shard_map/all_gather | solution.py:125
  373.8 93.2 %all-gather.15.cloned.1.call-done = bf16[1408,2048]{1,0:T(8,128)(2,1)} async-done(((bf16[1408,256]{1,0:T(8,128)(2,1)}), bf16[1408,2048]{1,0:T(8,128)(2,1)}) %all-gather.15.cloned.1.call-update) | async-done | bytes 5767184 | tf_op jit(solution)/shard_map/all_gather | solution.py:126
  467.0 20.6 %convolution_convert_fusion = bf16[1024,2048]{1,0:T(8,128)(2,1)} fusion(bf16[1408,2048]{1,0:T(8,128)(2,1)} %all-gather.15.cloned.1.call-done, f32[1024,1408]{1,0:T(8,128)} %fusion.74, bf16[1024,2048]{1,0:T(8,128)(2,1)} %all-gather.9.cloned.1.call-done, bf16[2048,1408]{1,0:T(8,128)(2,1)} %all-gather.13.cloned.1.call-done), kind=kOutput, calls=%fused_computation.80 | convolution fusion | flops 11821907968 | bytes 25690112 | tf_op jit(solution)/shard_map/dot_general | solution.py:196
  487.6 42.7 %reduce-scatter.5.cloned.1.call-done = bf16[1024,512]{1,0:T(8,128)(2,1)} async-done(((bf16[1024,2048]{1,0:T(8,128)(2,1)}), bf16[1024,512]{1,0:T(8,128)(2,1)}) %reduce-scatter.5.cloned.1.call-update) | async-done | bytes 1048592 | tf_op jit(solution)/shard_map/reduce_scatter | solution.py:197
  530.3 3.0 fusion.57
  (114 shorter events, 2.6 us)
Async XLA Ops:
  6.5 96.7 %copy-start = (bf16[512,2048]{1,0:T(8,128)(2,1)S(1)}, bf16[512,2048]{1,0:T(8,128)(2,1)}, u32[]{:S(2)}) copy-start(bf16[512,2048]{1,0:T(8,128)(2,1)} %param.27) | copy-start | bytes 6291460
  6.5 83.2 %all-gather.17.cloned.1.call-start = ((), (), s32[]{:S(2)}) async-start(), calls=%async_computation.8 | async-start | bytes 2359296 | tf_op jit(solution)/shard_map/all_gather | solution.py:13
  8.0 6.1 %copy-start.8 = (bf16[1024,256]{0,1:T(8,128)(2,1)}, bf16[1024,256]{0,1:T(8,128)(2,1)S(1)}, u32[]{:S(2)}) copy-start(bf16[1024,256]{0,1:T(8,128)(2,1)S(1)} %copy.44) | copy-start | bytes 1572868
  17.0 1.6 copy-start.14
  17.0 1.6 copy-start.13
  17.0 1.6 copy-start.15
  18.6 19.2 %copy-start.17 = (u32[32]{0:T(128)S(1)}, u32[32]{0:T(128)}, u32[]{:S(2)}) copy-start(u32[32]{0:T(128)} %constant.100) | copy-start | bytes 388
  20.8 1.7 copy-start.3
  22.5 2.7 copy-start.4
  22.5 2.7 copy-start.10
  26.3 1.4 copy-start.11
  30.0 1.7 copy-start.3
  31.7 2.7 copy-start.4
  31.7 2.7 copy-start.10
  35.5 1.4 copy-start.11
  37.0 0.7 copy-start.2
  37.8 113.0 %reduce-scatter.3.cloned.1.call-start = ((), (), s32[]{:S(2)}) async-start(), calls=%async_computation.2 | async-start | bytes 5242880 | tf_op jit(solution)/shard_map/reduce_scatter | solution.py:180
  67.1 4.2 copy-start.12
  73.2 2.9 copy-start.16
  89.8 9.2 %copy-start.9 = (bf16[1024,256]{0,1:T(8,128)(2,1)S(1)}, bf16[1024,256]{0,1:T(8,128)(2,1)}, u32[]{:S(2)}) copy-start(bf16[1024,256]{0,1:T(8,128)(2,1)} %copy-done.8) | copy-start | bytes 1572868
  99.0 3.9 copy-start.7
  107.6 43.1 %copy-start.5 = (bf16[1024,512]{1,0:T(8,128)(2,1)S(1)}, bf16[1024,512]{1,0:T(8,128)(2,1)}, u32[]{:S(2)}) copy-start(bf16[1024,512]{1,0:T(8,128)(2,1)} %param.25) | copy-start | bytes 3145732
  107.7 137.6 %all-gather.11.cloned.1.call-start = ((), (), s32[]{:S(2)}) async-start(), calls=%async_computation.4 | async-start | bytes 6488064 | tf_op jit(solution)/shard_map/all_gather | solution.py:124
  108.4 171.0 %all-gather.9.cloned.1.call-start = ((), (), s32[]{:S(2)}) async-start(), calls=%async_computation.3 | async-start | bytes 5242880 | tf_op jit(solution)/shard_map/all_gather | solution.py:190
  150.8 7.5 %copy-start.6 = (bf16[1024,512]{1,0:T(8,128)(2,1)S(1)}, bf16[1024,512]{1,0:T(8,128)(2,1)}, u32[]{:S(2)}) copy-start(bf16[1024,512]{1,0:T(8,128)(2,1)} %reduce-scatter.3.cloned.1.call-done) | copy-start | bytes 3145732
  159.7 214.1 %all-gather.13.cloned.1.call-start = ((), (), s32[]{:S(2)}) async-start(), calls=%async_computation.5 | async-start | bytes 6488064 | tf_op jit(solution)/shard_map/all_gather | solution.py:125
  160.3 306.7 %all-gather.15.cloned.1.call-start = ((), (), s32[]{:S(2)}) async-start(), calls=%async_computation.6 | async-start | bytes 6488064 | tf_op jit(solution)/shard_map/all_gather | solution.py:126
  160.9 369.5 %reduce-scatter.5.cloned.1.call-start = ((), (), s32[]{:S(2)}) async-start(), calls=%async_computation.7 | async-start | bytes 5242880 | tf_op jit(solution)/shard_map/reduce_scatter | solution.py:197
  487.6 45.7 %copy-start.1 = (bf16[512,2048]{1,0:T(8,128)(2,1)S(1)}, bf16[512,2048]{1,0:T(8,128)(2,1)}, u32[]{:S(2)}) copy-start(bf16[512,2048]{1,0:T(8,128)(2,1)} %param.27) | copy-start | bytes 6291460
Sparse Core Ops, SparseCore 0:
  37.9 51.8 all-gather.16
  107.8 42.9 reduce-scatter.2
  153.0 92.2 all-gather.10
  246.7 32.6 all-gather.8
  281.4 92.3 all-gather.12
  375.7 91.3 all-gather.14
  487.7 42.5 reduce-scatter.4
where the time goes:
time: 541 us; the launch traced here: 540 us
  waiting for transfers between devices  394 us (73%)
  matrix products  53.6 us (10%)
  blocking collectives  29.1 us (5%)
  other arithmetic  25.1 us (5%)
  local copies, waits for them, and re-layouts  23.3 us (4%)
  between operations  14.3 us (3%)
    all_gather x1, waiting for transfers between devices, local(): lax.all_gather(down_projection_weight, 'sp', axis=1, tiled=True)  93.2 us
    all_gather x1, waiting for transfers between devices, local(): lax.all_gather(gate_projection_weight, 'sp', axis=0, tiled=True)  84.2 us
    all_gather x1, waiting for transfers between devices, local(): lax.all_gather(up_projection_weight, 'sp', axis=0, tiled=True)  82.7 us
    reduce_scatter x1, waiting for transfers between devices, local(): lax.psum_scatter(down_terms.astype(jnp.bfloat16), 'tp', scatter_dimension...  42.7 us
    reduce_scatter x1, waiting for transfers between devices, local(): lax.psum_scatter(partial_value, 'tp', scatter_dimension=1, tiled=True)  41.6 us
    all_gather x1, waiting for transfers between devices, local(): lax.all_gather((stream_local * scale * gain_columns).astype(jnp.bfloat16)...  34.1 us
    unnamed x1, blocking collectives  23.3 us
    dot_general x1, matrix products, local(): down_terms = jnp.dot(hidden, whole_down, preferred_element_type=jnp.float32)  20.6 us
  transfers between devices with their start and end apart: 7, of which 7 were waited for; matrix products, arithmetic and copies ran while one was open for 6% of the time, Pallas kernels for 0%

commit v1 on v0

--- a/solution.py
+++ b/solution.py
@@ -120,9 +120,27 @@
     up_projection_weight,
     down_projection_weight,
 ):
+
+    def _put_cards(slab_in):
+        left_arr, y1, u_next = (lax.axis_size("sp"), lax.axis_index("sp"), slab_in.shape[0])
+        entries = [pp * left_arr if to_i == 0 else pp for to_i, pp in enumerate(slab_in.shape)]
+        k0 = 1
+        val2 = lax.dynamic_update_slice_in_dim(
+            jnp.zeros(entries, slab_in.dtype), slab_in, y1 * u_next, axis=0
+        )
+        while k0 < left_arr:
+            slab_in = lax.ppermute(
+                slab_in, "sp", [(to_i, (to_i + 1) % left_arr) for to_i in range(left_arr)]
+            )
+            val2 = lax.dynamic_update_slice_in_dim(
+                val2, slab_in, (y1 - k0) % left_arr * u_next, axis=0
+            )
+            k0 += 1
+        return val2
+
     whole_gate, whole_up, whole_down = (
         lax.all_gather(gate_projection_weight, "sp", axis=0, tiled=True),
-        lax.all_gather(up_projection_weight, "sp", axis=0, tiled=True),
+        _put_cards(up_projection_weight),
         lax.all_gather(down_projection_weight, "sp", axis=1, tiled=True),
     )
     token_rows = queries.shape[0]

time: 541 us -> 508 us (0.939)
  waiting for transfers between devices: 394 us -> 342 us
  local copies, waits for them, and re-layouts: 23.3 us -> 39.3 us
    ppermute x0 -> x7, waiting for transfers between devices: none -> 174 us  [_put_cards(): lax.ppermute(slab_in, 'sp', [(to_i, (to_i + 1) % left_arr) for to_i in ra...]
    all_gather x1, waiting for transfers between devices: 84.2 us -> 0.01 us  [local(): lax.all_gather(gate_projection_weight, 'sp', axis=0, tiled=True)]
    all_gather x1 -> x0, waiting for transfers between devices: 82.7 us -> none  [local(): lax.all_gather(up_projection_weight, 'sp', axis=0, tiled=True)]
    all_gather x1, waiting for transfers between devices: 34.1 us -> 0.01 us  [local(): lax.all_gather((stream_local * scale * gain_columns).astype(jnp.bfloat16)...]
    all_gather x1, waiting for transfers between devices: 93.2 us -> 70.8 us  [local(): lax.all_gather(down_projection_weight, 'sp', axis=1, tiled=True)]
    dynamic_update_slice x0 -> x8, local copies, waits for them, and re-layouts: none -> 9.64 us  [the longest x7 8.72 us: _put_cards(): lax.dynamic_update_slice_in_dim(val2, slab_in, (y1 - k0) % left_arr * u_n...]
  transfers between devices with their start and end apart: 7 -> 13, of which waited for: 7 -> 11; matrix products, arithmetic and copies ran while one was open for 6% -> 9% of each run, Pallas kernels for 0% -> 0%
where the time goes in v1:
time: 508 us; the launch traced here: 507 us
  waiting for transfers between devices  342 us (67%)
  matrix products  53.5 us (11%)
  local copies, waits for them, and re-layouts  39.3 us (8%)
  blocking collectives  29.1 us (6%)
  other arithmetic  26.3 us (5%)
  between operations  14.3 us (3%)
    ppermute x7, waiting for transfers between devices, _put_cards(): lax.ppermute(slab_in, 'sp', [(to_i, (to_i + 1) % left_arr) for to_i in ra...  174 us
    all_gather x1, waiting for transfers between devices, local(): lax.all_gather(down_projection_weight, 'sp', axis=1, tiled=True)  70.8 us
    reduce_scatter x1, waiting for transfers between devices, local(): lax.psum_scatter(down_terms.astype(jnp.bfloat16), 'tp', scatter_dimension...  42.7 us
    reduce_scatter x1, waiting for transfers between devices, local(): lax.psum_scatter(partial_value, 'tp', scatter_dimension=1, tiled=True)  41.6 us
    unnamed x1, blocking collectives  23.3 us
    dot_general x1, matrix products, local(): down_terms = jnp.dot(hidden, whole_down, preferred_element_type=jnp.float32)  20.5 us
    all_gather x1, waiting for transfers between devices, entering(): everything = jax.tree.map(lambda part: lax.all_gather(part, axis), array)  12.5 us
    dot_general x1, matrix products, local(): gate_value = jnp.dot(normed, whole_gate, preferred_element_type=jnp.float32)  11.7 us
  transfers between devices with their start and end apart: 13, of which 11 were waited for; matrix products, arithmetic and copies ran while one was open for 9% of the time, Pallas kernels for 0%

profile of v1, /device:TPU:0, one launch (start us, length us, event | category | flops | bytes accessed | tf_op | source)
XLA Modules:
  0.0 507.3 jit_solution(16893732362691284882)
XLA Ops:
  6.6 1.4 copy.44
  8.0 1.0 copy.45
  9.0 2.3 copy.42
  11.2 2.8 convert_bitcast_fusion
  14.1 2.9 copy.43
  17.0 2.1 copy.40
  19.0 1.3 copy.41
  20.4 18.4 %while.37 = (s32[]{:T(128)}, f32[2,128,256]{2,1,0:T(8,128)S(1)}, f32[2]{0:T(128)S(1)}, f32[2]{0:T(128)S(1)}, f32[2,2,512,256]{3,2,1,0:T(8,128)}, /*index=5*/f32[...) while((s32[]{:T(128)}, f32[2,128,256]{2,1,0:T(8,128)S(1)}, ...), condition=%wide.region_5.6_spmd.clone, body=%wide.region_0.5_spmd.clone.sunk | while | flops 2557093888 | bytes 39478384 | solution.py:87
  22.8 1.5 fusion.120
  24.3 2.6 fusion.122
  27.0 1.1 fusion.123
  28.2 1.3 convolution_add_fusion.2
  32.0 1.5 fusion.120
  33.5 2.6 fusion.122
  36.2 1.1 fusion.123
  37.4 1.3 convolution_add_fusion.2
  38.8 0.7 copy-done.2
  41.2 23.3 %all-reduce.2 = (f32[16]{0:T(128)S(1)}, f32[16]{0:T(128)S(1)}) all-reduce(f32[16]{0:T(128)S(1)} %dynamic-update-slice, f32[16]{0:T(128)S(1)} %dynamic-update-slice.1), channel_id=2, replica_groups=mesh['sp'=8,'tp'=4] {'sp'}, use_global_device_ids=true, to_apply=%add | all-reduce | flops 32 | bytes 256
  64.7 4.2 copy.49
  68.9 4.1 reshape.321
  73.0 3.2 add_divide_fusion
  76.1 2.9 copy.52
  79.1 12.5 %all-gather.14.cloned.1.call-done = f32[16,128,256]{2,1,0:T(8,128)} async-done(((f32[2,128,256]{2,1,0:T(8,128)}), f32[16,128,256]{2,1,0:T(8,128)}) %all-gather.14.cloned.1.call-update) | async-done | bytes 2097168 | tf_op jit(solution)/shard_map/all_gather | solution.py:13
  91.6 9.1 %while.38 = (s32[]{:T(128)}, f32[2,128,256]{2,1,0:T(8,128)S(1)}, f32[2]{0:T(128)S(1)}, s32[]{:T(128)}, f32[8,2]{1,0:T(8,128)S(1)}, /*index=5*/f32[8,2]{1,0:T(8,1...) while((s32[]{:T(128)}, f32[2,128,256]{2,1,0:T(8,128)S(1)}, f32[2]{0:T(128)S(1)}, s32[]{:T(128)}, ...), condition=%wide.region_7.8_spmd.clone, body=%wide.region_6.7_spmd.clone.sunk | while | flops 327698 | bytes 786647 | solution.py:25
  91.6 1.1 fusion.124
  92.8 1.1 fusion.124
  93.9 1.1 fusion.124
  95.1 1.1 fusion.124
  96.2 1.1 fusion.124
  97.3 1.1 fusion.124
  98.4 1.1 fusion.124
  99.6 1.1 fusion.124
  100.8 3.9 fusion.58
  105.0 4.4 convolution_convert_fusion.1
  109.5 0.7 all-gather.10.cloned.1.call-update
  110.2 0.8 dynamic-slice_convert_fusion
  111.0 41.6 %reduce-scatter.3.cloned.1.call-done = bf16[1024,512]{1,0:T(8,128)(2,1)} async-done(((bf16[1024,2048]{1,0:T(8,128)(2,1)}), bf16[1024,512]{1,0:T(8,128)(2,1)}) %reduce-scatter.3.cloned.1.call-update) | async-done | bytes 1048592 | tf_op jit(solution)/shard_map/reduce_scatter | solution.py:198
  152.6 1.7 fusion.54
  154.3 5.8 %psum.7 = f32[1024]{0:T(1024)S(1)} all-reduce(f32[1024]{0:T(1024)S(1)} %fusion.54), channel_id=1, replica_groups=mesh['sp'=8,'tp'=4] {'tp'}, use_global_device_ids=true, to_apply=%region_11.12 | all-reduce | flops 1024 | bytes 8192 | tf_op jit(solution)/shard_map/psum | solution.py:203
  160.1 1.4 fusion.56
  162.1 1.7 collective-permute-start
  163.8 34.0 %collective-permute-done = bf16[256,1408]{1,0:T(8,128)(2,1)S(1)} collective-permute-done((bf16[256,1408]{1,0:T(8,128)(2,1)S(1)}, bf16[256,1408]{1,0:T(8,128)(2,1)S(1)}, u32[]{:S(2)}, u32[]{:S(2)}) %collective-permute-start) | collective-permute-done | bytes 720928 | tf_op jit(solution)/shard_map/ppermute | solution.py:132
  197.8 27.2 %collective-permute-done.1 = bf16[256,1408]{1,0:T(8,128)(2,1)S(1)} collective-permute-done((bf16[256,1408]{1,0:T(8,128)(2,1)S(1)}, bf16[256,1408]{1,0:T(8,128)(2,1)S(1)}, u32[]{:S(2)}, u32[]{:S(2)}) %collective-permute-start.1) | collective-permute-done | bytes 720928 | tf_op jit(solution)/shard_map/ppermute | solution.py:132
  225.0 0.9 copy-done.13
  225.9 36.5 %collective-permute-done.2 = bf16[256,1408]{1,0:T(8,128)(2,1)S(1)} collective-permute-done((bf16[256,1408]{1,0:T(8,128)(2,1)S(1)}, bf16[256,1408]{1,0:T(8,128)(2,1)S(1)}, u32[]{:S(2)}, u32[]{:S(2)}) %collective-permute-start.2) | collective-permute-done | bytes 720928 | tf_op jit(solution)/shard_map/ppermute | solution.py:132
  262.4 0.9 copy-done.15
  263.3 37.2 %collective-permute-done.3 = bf16[256,1408]{1,0:T(8,128)(2,1)} collective-permute-done((bf16[256,1408]{1,0:T(8,128)(2,1)S(1)}, bf16[256,1408]{1,0:T(8,128)(2,1)}, u32[]{:S(2)}, u32[]{:S(2)}) %collective-permute-start.3) | collective-permute-done | bytes 720928 | tf_op jit(solution)/shard_map/ppermute | solution.py:132
  300.5 2.9 broadcast_in_dim.38
  303.5 0.9 constant_dynamic-update-slice_fusion.7
  304.4 10.5 %collective-permute-done.4 = bf16[256,1408]{1,0:T(8,128)(2,1)} collective-permute-done((bf16[256,1408]{1,0:T(8,128)(2,1)}, bf16[256,1408]{1,0:T(8,128)(2,1)}, u32[]{:S(2)}, u32[]{:S(2)}) %collective-permute-start.4) | collective-permute-done | bytes 720928 | tf_op jit(solution)/shard_map/ppermute | solution.py:132
  314.8 0.9 constant_dynamic-update-slice_fusion.6
  315.8 0.9 constant_dynamic-update-slice_fusion.5
  316.7 0.9 constant_dynamic-update-slice_fusion.4
  317.7 15.7 %collective-permute-done.5 = bf16[256,1408]{1,0:T(8,128)(2,1)S(1)} collective-permute-done((bf16[256,1408]{1,0:T(8,128)(2,1)}, bf16[256,1408]{1,0:T(8,128)(2,1)S(1)}, u32[]{:S(2)}, u32[]{:S(2)}) %collective-permute-start.5) | collective-permute-done | bytes 720928 | tf_op jit(solution)/shard_map/ppermute | solution.py:132
  333.4 2.0 constant_dynamic-update-slice_fusion.3
  335.4 2.1 constant_dynamic-update-slice_fusion.2
  337.5 0.9 constant_dynamic-update-slice_fusion.1
  338.4 12.4 %collective-permute-done.6 = bf16[256,1408]{1,0:T(8,128)(2,1)S(1)} collective-permute-done((bf16[256,1408]{1,0:T(8,128)(2,1)S(1)}, bf16[256,1408]{1,0:T(8,128)(2,1)S(1)}, u32[]{:S(2)}, u32[]{:S(2)}) %collective-permute-start.6) | collective-permute-done | bytes 720928 | tf_op jit(solution)/shard_map/ppermute | solution.py:132
  350.8 0.9 constant_dynamic-update-slice_fusion
  351.7 11.7 %fusion.74 = f32[1024,1408]{1,0:T(8,128)} fusion(bf16[1024,2048]{1,0:T(8,128)(2,1)} %all-gather.8.cloned.1.call-done, bf16[2048,1408]{1,0:T(8,128)(2,1)} %all-gather.10.cloned.1.call-done), kind=kOutput, calls=%fused_computation.125 | convolution fusion | flops 5905580032 | bytes 15728640 | tf_op jit(solution)/shard_map/dot_general | solution.py:211
  363.4 70.8 %all-gather.12.cloned.1.call-done = bf16[1408,2048]{1,0:T(8,128)(2,1)} async-done(((bf16[1408,256]{1,0:T(8,128)(2,1)}), bf16[1408,2048]{1,0:T(8,128)(2,1)}) %all-gather.12.cloned.1.call-update) | async-done | bytes 5767184 | tf_op jit(solution)/shard_map/all_gather | solution.py:144
  434.2 20.5 %convolution_convert_fusion = bf16[1024,2048]{1,0:T(8,128)(2,1)} fusion(bf16[1408,2048]{1,0:T(8,128)(2,1)} %all-gather.12.cloned.1.call-done, f32[1024,1408]{1,0:T(8,128)} %fusion.74, bf16[1024,2048]{1,0:T(8,128)(2,1)} %all-gather.8.cloned.1.call-done, bf16[2048,1408]{1,0:T(8,128)(2,1)} %constant_dynamic-update-slice_fusion), kind=kOutput, calls=%fused_computation.80 | convolution fusion | flops 11821907968 | bytes 25690112 | tf_op jit(solution)/shard_map/dot_general | solution.py:214
  454.8 42.7 %reduce-scatter.5.cloned.1.call-done = bf16[1024,512]{1,0:T(8,128)(2,1)} async-done(((bf16[1024,2048]{1,0:T(8,128)(2,1)}), bf16[1024,512]{1,0:T(8,128)(2,1)}) %reduce-scatter.5.cloned.1.call-update) | async-done | bytes 1048592 | tf_op jit(solution)/shard_map/reduce_scatter | solution.py:215
  497.5 3.0 fusion.57
  (142 shorter events, 8.0 us)
Async XLA Ops:
  6.5 98.5 %copy-start = (bf16[512,2048]{1,0:T(8,128)(2,1)S(1)}, bf16[512,2048]{1,0:T(8,128)(2,1)}, u32[]{:S(2)}) copy-start(bf16[512,2048]{1,0:T(8,128)(2,1)} %param.27) | copy-start | bytes 6291460
  6.5 85.0 %all-gather.14.cloned.1.call-start = ((), (), s32[]{:S(2)}) async-start(), calls=%async_computation.7 | async-start | bytes 2359296 | tf_op jit(solution)/shard_map/all_gather | solution.py:13
  8.0 6.1 %copy-start.8 = (bf16[1024,256]{0,1:T(8,128)(2,1)}, bf16[1024,256]{0,1:T(8,128)(2,1)S(1)}, u32[]{:S(2)}) copy-start(bf16[1024,256]{0,1:T(8,128)(2,1)S(1)} %copy.44) | copy-start | bytes 1572868
  16.9 3.4 copy-start.18
  16.9 3.4 copy-start.17
  16.9 3.4 copy-start.19
  20.4 19.2 %copy-start.21 = (u32[32]{0:T(128)S(1)}, u32[32]{0:T(128)}, u32[]{:S(2)}) copy-start(u32[32]{0:T(128)} %constant.161) | copy-start | bytes 388
  22.7 1.7 copy-start.3
  24.3 2.7 copy-start.4
  24.3 2.7 copy-start.10
  28.1 1.4 copy-start.11
  31.8 1.7 copy-start.3
  33.5 2.7 copy-start.4
  33.5 2.7 copy-start.10
  37.3 1.4 copy-start.11
  38.8 0.7 copy-start.2
  39.6 113.0 %reduce-scatter.3.cloned.1.call-start = ((), (), s32[]{:S(2)}) async-start(), calls=%async_computation.2 | async-start | bytes 5242880 | tf_op jit(solution)/shard_map/reduce_scatter | solution.py:198
  76.1 2.9 copy-start.20
  91.6 9.2 %copy-start.9 = (bf16[1024,256]{0,1:T(8,128)(2,1)S(1)}, bf16[1024,256]{0,1:T(8,128)(2,1)}, u32[]{:S(2)}) copy-start(bf16[1024,256]{0,1:T(8,128)(2,1)} %copy-done.8) | copy-start | bytes 1572868
  100.8 3.9 copy-start.7
  109.4 43.1 %copy-start.5 = (bf16[1024,512]{1,0:T(8,128)(2,1)S(1)}, bf16[1024,512]{1,0:T(8,128)(2,1)}, u32[]{:S(2)}) copy-start(bf16[1024,512]{1,0:T(8,128)(2,1)} %param.25) | copy-start | bytes 3145732
  109.5 242.3 %all-gather.10.cloned.1.call-start = ((), (), s32[]{:S(2)}) async-start(), calls=%async_computation.4 | async-start | bytes 6488064 | tf_op jit(solution)/shard_map/all_gather | solution.py:142
  110.2 241.5 %all-gather.8.cloned.1.call-start = ((), (), s32[]{:S(2)}) async-start(), calls=%async_computation.3 | async-start | bytes 5242880 | tf_op jit(solution)/shard_map/all_gather | solution.py:208
  152.6 7.5 %copy-start.6 = (bf16[1024,512]{1,0:T(8,128)(2,1)S(1)}, bf16[1024,512]{1,0:T(8,128)(2,1)}, u32[]{:S(2)}) copy-start(bf16[1024,512]{1,0:T(8,128)(2,1)} %reduce-scatter.3.cloned.1.call-done) | copy-start | bytes 3145732
  160.1 2.0 copy-start.12
  161.5 272.7 %all-gather.12.cloned.1.call-start = ((), (), s32[]{:S(2)}) async-start(), calls=%async_computation.5 | async-start | bytes 6488064 | tf_op jit(solution)/shard_map/all_gather | solution.py:144
  162.1 335.4 %reduce-scatter.5.cloned.1.call-start = ((), (), s32[]{:S(2)}) async-start(), calls=%async_computation.6 | async-start | bytes 5242880 | tf_op jit(solution)/shard_map/reduce_scatter | solution.py:215
  162.1 35.7 %collective-permute-start = (bf16[256,1408]{1,0:T(8,128)(2,1)S(1)}, bf16[256,1408]{1,0:T(8,128)(2,1)S(1)}, u32[]{:S(2)}, u32[]{:S(2)}) collective-permute-start(bf16[256,1408]{1,0:T(8,128)(2,1)S(1)} %copy-done.12), channel_id=1, source_target_pairs={{0,4},{4,8},{8,12},{12,16},{16,20},{20,24},{24,28},{28,0},{1,5},{5... | collective-permute-start | bytes 2162696 | tf_op jit(solution)/shard_map/ppermute | solution.py:132
  197.8 27.2 %collective-permute-start.1 = (bf16[256,1408]{1,0:T(8,128)(2,1)S(1)}, bf16[256,1408]{1,0:T(8,128)(2,1)S(1)}, u32[]{:S(2)}, u32[]{:S(2)}) collective-permute-start(bf16[256,1408]{1,0:T(8,128)(2,1)S(1)} %collective-permute-done), channel_id=1, source_target_pairs={{0,4},{4,8},{8,12},{12,16},{16,20},{20,24},{24,28},{28,0},{1,5},{5... | collective-permute-start | bytes 2162696 | tf_op jit(solution)/shard_map/ppermute | solution.py:132
  225.0 0.9 copy-start.13
  225.9 36.5 %collective-permute-start.2 = (bf16[256,1408]{1,0:T(8,128)(2,1)S(1)}, bf16[256,1408]{1,0:T(8,128)(2,1)S(1)}, u32[]{:S(2)}, u32[]{:S(2)}) collective-permute-start(bf16[256,1408]{1,0:T(8,128)(2,1)S(1)} %collective-permute-done.1), channel_id=1, source_target_pairs={{0,4},{4,8},{8,12},{12,16},{16,20},{20,24},{24,28},{28,0},{1,5},{5... | collective-permute-start | bytes 2162696 | tf_op jit(solution)/shard_map/ppermute | solution.py:132
  262.4 0.9 copy-start.15
  263.3 37.3 %collective-permute-start.3 = (bf16[256,1408]{1,0:T(8,128)(2,1)S(1)}, bf16[256,1408]{1,0:T(8,128)(2,1)}, u32[]{:S(2)}, u32[]{:S(2)}) collective-permute-start(bf16[256,1408]{1,0:T(8,128)(2,1)S(1)} %collective-permute-done.2), channel_id=1, source_target_pairs={{0,4},{4,8},{8,12},{12,16},{16,20},{20,24},{24,28},{28,0},{1,5},{5... | collective-permute-start | bytes 2162696 | tf_op jit(solution)/shard_map/ppermute | solution.py:132
  300.5 14.3 %collective-permute-start.4 = (bf16[256,1408]{1,0:T(8,128)(2,1)}, bf16[256,1408]{1,0:T(8,128)(2,1)}, u32[]{:S(2)}, u32[]{:S(2)}) collective-permute-start(bf16[256,1408]{1,0:T(8,128)(2,1)} %collective-permute-done.3), channel_id=1, source_target_pairs={{0,4},{4,8},{8,12},{12,16},{16,20},{20,24},{24,28},{28,0},{1,5},{5... | collective-permute-start | bytes 2162696 | tf_op jit(solution)/shard_map/ppermute | solution.py:132
  303.4 12.3 %copy-start.14 = (bf16[256,1408]{1,0:T(8,128)(2,1)S(1)}, bf16[256,1408]{1,0:T(8,128)(2,1)}, u32[]{:S(2)}) copy-start(bf16[256,1408]{1,0:T(8,128)(2,1)} %copy-done.13) | copy-start | bytes 2162692
  303.4 13.3 %copy-start.16 = (bf16[256,1408]{1,0:T(8,128)(2,1)S(1)}, bf16[256,1408]{1,0:T(8,128)(2,1)}, u32[]{:S(2)}) copy-start(bf16[256,1408]{1,0:T(8,128)(2,1)} %copy-done.15) | copy-start | bytes 2162692
  314.8 18.5 %collective-permute-start.5 = (bf16[256,1408]{1,0:T(8,128)(2,1)}, bf16[256,1408]{1,0:T(8,128)(2,1)S(1)}, u32[]{:S(2)}, u32[]{:S(2)}) collective-permute-start(bf16[256,1408]{1,0:T(8,128)(2,1)} %collective-permute-done.4), channel_id=1, source_target_pairs={{0,4},{4,8},{8,12},{12,16},{16,20},{20,24},{24,28},{28,0},{1,5},{5... | collective-permute-start | bytes 2162696 | tf_op jit(solution)/shard_map/ppermute | solution.py:132
  333.4 17.5 %collective-permute-start.6 = (bf16[256,1408]{1,0:T(8,128)(2,1)S(1)}, bf16[256,1408]{1,0:T(8,128)(2,1)S(1)}, u32[]{:S(2)}, u32[]{:S(2)}) collective-permute-start(bf16[256,1408]{1,0:T(8,128)(2,1)S(1)} %collective-permute-done.5), channel_id=1, source_target_pairs={{0,4},{4,8},{8,12},{12,16},{16,20},{20,24},{24,28},{28,0},{1,5},{5... | collective-permute-start | bytes 2162696 | tf_op jit(solution)/shard_map/ppermute | solution.py:132
  454.8 45.7 %copy-start.1 = (bf16[512,2048]{1,0:T(8,128)(2,1)S(1)}, bf16[512,2048]{1,0:T(8,128)(2,1)}, u32[]{:S(2)}) copy-start(bf16[512,2048]{1,0:T(8,128)(2,1)} %param.27) | copy-start | bytes 6291460
Sparse Core Ops, SparseCore 0:
  39.7 51.8 all-gather.13
  109.6 42.9 reduce-scatter.2
  154.7 130.4 all-gather.9
  286.6 52.4 all-gather.7
  341.0 93.1 all-gather.11
  454.9 42.5 reduce-scatter.4
